TPU v7x, 32 devices: a whole 2x2x4 slice. The times are simulated.
32 devices in a mesh: fs: 16 (over z, y, x), tp: 2 (over core).
Axes of the slice: x: 2, y: 2, z: 4, core: 2. Of those that a mesh axis runs over, the one named last changes fastest.
Arguments:
- tokens: bfloat16 [4096, 2048], P('fs'), may hold values from -6 to 6
- routes: int32 [4096, 6], P('fs'), may hold values from 0 to 15, all different within a row; in each aligned block of 256 rows (0 to 255, 256 to 511, ...) at most 160 rows name the same one
- route_weights: float32 [4096, 6], P('fs'), may hold values from 0.1 to 1
- norm_gain: float32 [2048], P('fs'), may hold values from 0.1 to 1.9
- expert_gate: float32 [16, 2048, 1024], P(None, 'fs', 'tp'), may hold values from -0.125 to 0.125
- expert_up: float32 [16, 2048, 1024], P(None, 'fs', 'tp'), may hold values from -0.125 to 0.125
- expert_down: float32 [16, 2048, 1024], P(None, 'fs', 'tp'), may hold values from -0.1875 to 0.1875
- shared_gate: float32 [2048, 1024], P('fs', 'tp'), may hold values from -0.125 to 0.125
- shared_up: float32 [2048, 1024], P('fs', 'tp'), may hold values from -0.125 to 0.125
- shared_down: float32 [2048, 1024], P('fs', 'tp'), may hold values from -0.1875 to 0.1875
Outputs:
- layer_output: bfloat16 [4096, 2048], P('fs', 'tp')
- sample_gate: bfloat16 [16, 2048, 1024], P('fs', None, 'tp')
- sample_up: bfloat16 [16, 2048, 1024], P('fs', None, 'tp')
- sample_down: bfloat16 [16, 2048, 1024], P('fs', None, 'tp')
- common_gate: bfloat16 [2048, 1024], P(None, 'tp')
- common_up: bfloat16 [2048, 1024], P(None, 'tp')
- common_down: bfloat16 [2048, 1024], P(None, 'tp')
Inputs may be any that keep to these rules, and one draw needn't show every extreme that they name: `routes`: each row names 6 different experts. In each aligned block of 256 rows (the rows of one index of fs) no expert is named by more than 160 rows, a bound that some expert reaches in some blocks.
All inputs are finite; a program needn't handle non-finite values.
Results may differ from a plain program's by a relative error of at most 0.015.
Values may be sent and summed in bfloat16 or wider, within the bound.
A program may use at most 128 MiB of HBM per device.

v0:
```python
import jax
import jax.numpy as jnp
from jax import lax
from jax.sharding import PartitionSpec as P

EPSILON = 1e-06


def normalize(tokens):
    values = tokens.astype(jnp.float32)
    scale = lax.rsqrt(jnp.mean(values * values, axis=-1, keepdims=True) + EPSILON)
    return (values * scale).astype(jnp.bfloat16)


def slot_table(routes, experts, capacity):
    flat_route = routes.reshape(-1)
    member = (flat_route[:, None] == jnp.arange(experts, dtype=jnp.int32)[None, :]).astype(
        jnp.int32
    )
    before = jnp.sum((jnp.cumsum(member, axis=0) - member) * member, axis=1)
    return flat_route * capacity + before


def body(
    tokens,
    routes,
    route_weights,
    norm_gain,
    expert_gate,
    expert_up,
    expert_down,
    shared_gate,
    shared_up,
    shared_down,
):
    gain_rows = norm_gain[None, :, None]
    rounded = (
        (expert_gate * gain_rows).astype(jnp.bfloat16),
        (expert_up * gain_rows).astype(jnp.bfloat16),
        expert_down.astype(jnp.bfloat16),
    )
    sample_gate, sample_up, sample_down = (
        lax.all_to_all(rounded[0], "fs", split_axis=0, concat_axis=1, tiled=True),
        lax.all_to_all(rounded[1], "fs", split_axis=0, concat_axis=1, tiled=True),
        lax.all_to_all(rounded[2], "fs", split_axis=0, concat_axis=1, tiled=True),
    )
    gate_rows = sample_gate[0]
    up_rows = sample_up[0]
    down_rows = sample_down[0]
    normed = normalize(tokens)
    tok_rows, width = normed.shape
    picks = routes.shape[1]
    experts = expert_gate.shape[0]
    tp_count = lax.axis_size("tp")
    capacity = min(tok_rows, tp_count * max(1, tok_rows * picks * 5 // (3 * experts * tp_count)))
    slots = slot_table(routes, experts, capacity)
    sources = (
        jnp.full((experts * capacity,), tok_rows, jnp.int32)
        .at[slots]
        .set(jnp.arange(tok_rows * picks, dtype=jnp.int32) // picks)
    )
    padded = jnp.concatenate([normed, jnp.zeros((1, width), jnp.bfloat16)], axis=0)
    outgoing = padded[sources].reshape(experts, capacity, width)
    shared_rounded = (
        (shared_gate * norm_gain[:, None]).astype(jnp.bfloat16),
        (shared_up * norm_gain[:, None]).astype(jnp.bfloat16),
        shared_down.astype(jnp.bfloat16),
    )
    common_gate, common_up, common_down = (
        lax.all_gather(shared_rounded[0], "fs", axis=0, tiled=True),
        lax.all_gather(shared_rounded[1], "fs", axis=0, tiled=True),
        lax.all_gather(shared_rounded[2], "fs", axis=0, tiled=True),
    )
    shared_gate_act = jnp.dot(normed, common_gate, preferred_element_type=jnp.float32)
    shared_up_act = jnp.dot(normed, common_up, preferred_element_type=jnp.float32)
    shared_hidden = (jax.nn.silu(shared_gate_act) * shared_up_act).astype(jnp.bfloat16)
    shared_terms = jnp.einsum(
        "th,dh->td", shared_hidden, common_down, preferred_element_type=jnp.float32
    )
    share = capacity // tp_count
    whole_gate, whole_up, whole_down = (
        lax.all_gather(gate_rows, "tp", axis=1, tiled=True),
        lax.all_gather(up_rows, "tp", axis=1, tiled=True),
        lax.all_gather(down_rows, "tp", axis=1, tiled=True),
    )
    own_share = lax.dynamic_slice_in_dim(outgoing, lax.axis_index("tp") * share, share, 1)
    block = lax.all_to_all(own_share, "fs", split_axis=0, concat_axis=0, tiled=True)
    flat = block.reshape(-1, width)
    gate = jnp.dot(flat, whole_gate, preferred_element_type=jnp.float32)
    upward = jnp.dot(flat, whole_up, preferred_element_type=jnp.float32)
    hidden = (jax.nn.silu(gate) * upward).astype(jnp.bfloat16)
    parts = jnp.einsum(
        "rbf,dbf->rbd",
        hidden.reshape(flat.shape[0], tp_count, -1),
        whole_down.reshape(width, tp_count, -1),
        preferred_element_type=jnp.float32,
    ).astype(jnp.bfloat16)
    parts = lax.optimization_barrier(parts)
    total = jnp.sum(parts.astype(jnp.float32), axis=1).astype(jnp.bfloat16)
    results = total.reshape(block.shape[0], block.shape[1], width)
    back = lax.all_to_all(results, "fs", split_axis=0, concat_axis=0, tiled=True).reshape(
        experts * share, width
    )
    position = slots % capacity
    owner = position // share
    local = slots // capacity * share + position % share
    taken = back[local].astype(jnp.float32).reshape(tok_rows, picks, width)
    keep = (owner == lax.axis_index("tp")).astype(jnp.float32).reshape(tok_rows, picks)
    routed_part = jnp.sum(taken * (route_weights * keep)[:, :, None], axis=1)
    shared_part = lax.optimization_barrier(shared_terms.astype(jnp.bfloat16)).astype(jnp.float32)
    layer_output = lax.psum_scatter(
        (routed_part + shared_part).astype(jnp.bfloat16), "tp", scatter_dimension=1, tiled=True
    )
    return (layer_output, sample_gate, sample_up, sample_down, common_gate, common_up, common_down)


def solution(mesh):
    return jax.shard_map(
        body,
        mesh=mesh,
        in_specs=(
            P("fs", None),
            P("fs", None),
            P("fs", None),
            P("fs"),
            P(None, "fs", "tp"),
            P(None, "fs", "tp"),
            P(None, "fs", "tp"),
            P("fs", "tp"),
            P("fs", "tp"),
            P("fs", "tp"),
        ),
        out_specs=(
            P("fs", "tp"),
            P("fs", None, "tp"),
            P("fs", None, "tp"),
            P("fs", None, "tp"),
            P(None, "tp"),
            P(None, "tp"),
            P(None, "tp"),
        ),
        check_vma=False,
    )
```

profile of v0, /device:TPU:0, one launch (start us, length us, event | category | flops | bytes accessed | tf_op | source)
XLA Modules:
  0.0 618.7 jit_solution(1220370238295980275)
XLA Ops:
  7.2 6.1 multiply_convert_fusion.1
  13.3 57.0 %all_to_all.46 = bf16[16,128,512]{2,1,0:T(8,128)(2,1)} all-to-all(bf16[16,128,512]{2,1,0:T(8,128)(2,1)S(1)} %get-tuple-element.12), channel_id=1, replica_groups=mesh['fs'=16,'tp'=2] {'fs'}, dimensions={0} | all-to-all | bytes 4194304 | tf_op jit(solution)/shard_map/all_to_all | solution.py:43
  70.3 3.9 all-to-all-start.2
  78.1 38.7 %all-to-all-done.2 = bf16[16,128,512]{2,1,0:T(8,128)(2,1)S(1)} async-done(((bf16[16,128,512]{2,1,0:T(8,128)(2,1)}), bf16[16,128,512]{2,1,0:T(8,128)(2,1)S(1)}, u32[]{:S(2)}, u32[]{:S(2)}) %all-to-all-start.2) | async-done | bytes 2097184 | tf_op jit(solution)/shard_map/all_to_all | solution.py:44
  116.8 9.9 %all-to-all-start.3 = ((bf16[16,128,512]{2,1,0:T(8,128)(2,1)}), bf16[16,128,512]{2,1,0:T(8,128)(2,1)}, u32[]{:S(2)}, u32[]{:S(2)}) async-start(bf16[16,128,512]{2,1,0:T(8,128)(2,1)} %convert_element_type.70), calls=%async_computation.3 | async-start | bytes 4194304 | tf_op jit(solution)/shard_map/all_to_all | solution.py:45
  127.5 4.6 reduce-window.6
  133.9 6.2 %scatter_custom_fusion = s32[2560]{0:T(1024)S(1)} fusion(s32[1536]{0:T(1024)S(1)} %get-tuple-element.8, s32[1536]{0:T(1024)S(1)} %add_select_fusion.2, s32[]{:T(128)} %constant.63.clone.1), kind=kCustom, calls=%fused_computation.62 | custom fusion | bytes 10244 | tf_op jit(solution)/shard_map/scatter | solution.py:60
  140.1 10.8 %gather_fusion = bf16[2560,2048]{1,0:T(8,128)(2,1)} fusion(bf16[257,2048]{1,0:T(8,128)(2,1)S(1)} %concatenate.3, s32[3072]{0:T(1024)S(1)} %pad_clamp_fusion), kind=kCustom, calls=%fused_computation | custom fusion | bytes 20981760 | tf_op jit(solution)/shard_map/gather | solution.py:63
  150.9 5.7 constant_dynamic-slice_fusion
  156.6 12.7 %all-to-all-done.3 = bf16[16,128,512]{2,1,0:T(8,128)(2,1)} async-done(((bf16[16,128,512]{2,1,0:T(8,128)(2,1)}), bf16[16,128,512]{2,1,0:T(8,128)(2,1)}, u32[]{:S(2)}, u32[]{:S(2)}) %all-to-all-start.3) | async-done | bytes 2097184 | tf_op jit(solution)/shard_map/all_to_all | solution.py:45
  169.3 9.8 %all-to-all-start = ((bf16[16,80,2048]{2,1,0:T(8,128)(2,1)}), bf16[16,80,2048]{2,1,0:T(8,128)(2,1)}, u32[]{:S(2)}, u32[]{:S(2)}) async-start(bf16[16,80,2048]{2,1,0:T(8,128)(2,1)} %constant_dynamic-slice_fusion), calls=%async_computation | async-start | bytes 10485760 | tf_op jit(solution)/shard_map/all_to_all | solution.py:87
  180.0 3.9 copy.39
  185.0 99.7 %all-to-all-done = bf16[16,80,2048]{2,1,0:T(8,128)(2,1)} async-done(((bf16[16,80,2048]{2,1,0:T(8,128)(2,1)}), bf16[16,80,2048]{2,1,0:T(8,128)(2,1)}, u32[]{:S(2)}, u32[]{:S(2)}) %all-to-all-start) | async-done | bytes 5242912 | tf_op jit(solution)/shard_map/all_to_all | solution.py:87
  284.7 10.6 %fusion.27 = f32[1280,1024]{0,1:T(8,128)} fusion(bf16[1280,2048]{1,0:T(8,128)(2,1)} %bitcast.2, bf16[2048,1024]{1,0:T(8,128)(2,1)} %all-gather.7.cloned.1.call-done), kind=kOutput, calls=%fused_computation.68 | convolution fusion | flops 5368709120 | bytes 14680064 | tf_op jit(solution)/shard_map/dot_general | solution.py:89
  295.3 11.6 %multiply_convert_fusion = bf16[1280,1024]{0,1:T(8,128)(2,1)} fusion(f32[1280,1024]{0,1:T(8,128)} %fusion.27, bf16[1280,2048]{1,0:T(8,128)(2,1)} %bitcast.2, bf16[2048,1024]{1,0:T(8,128)(2,1)} %all-gather.9.cloned.1.call-done), kind=kOutput, calls=%fused_computation.6 | convolution fusion | flops 5376573440 | bytes 17301504 | tf_op jit(solution)/shard_map/dot_general | solution.py:90
  306.9 10.9 %fusion = bf16[1280,2,2048]{2,0,1:T(8,128)(2,1)} fusion(bf16[1280,2,512]{0,2,1:T(8,128)(2,1)} %bitcast.52, bf16[2048,2,512]{0,2,1:T(8,128)(2,1)} %bitcast.51), kind=kOutput, calls=%fused_computation.5 | convolution fusion | flops 5373952000 | bytes 17301504 | tf_op jit(solution)/shard_map/rbf,dbf->rbd/dot_general | solution.py:92
  317.8 11.2 %reduce_sum.46 = bf16[1280,2048]{1,0:T(8,128)(2,1)} reduce(bf16[1280,2,2048]{2,0,1:T(8,128)(2,1)} %fusion, bf16[]{:T(256)} %constant.62.clone.1), dimensions={1}, to_apply=%region_5.6 | reduce | flops 2621440 | bytes 15728642 | tf_op jit(solution)/shard_map/reduce_sum | solution.py:99
  329.0 35.7 %all-to-all-start.4 = ((bf16[16,80,2048]{2,1,0:T(8,128)(2,1)}), bf16[16,80,2048]{2,1,0:T(8,128)(2,1)}, u32[]{:S(2)}, u32[]{:S(2)}) async-start(bf16[16,80,2048]{2,1,0:T(8,128)(2,1)} %bitcast.44), calls=%async_computation.4 | async-start | bytes 10485760 | tf_op jit(solution)/shard_map/all_to_all | solution.py:101
  368.9 120.3 %all-gather.15.cloned.1.call-done = bf16[2048,512]{1,0:T(8,128)(2,1)} async-done(((bf16[128,512]{1,0:T(8,128)(2,1)}), bf16[2048,512]{1,0:T(8,128)(2,1)}) %all-gather.15.cloned.1.call-update) | async-done | bytes 2097168 | tf_op jit(solution)/shard_map/all_gather | solution.py:71
  489.2 62.3 %all-gather.17.cloned.1.call-done = bf16[2048,512]{1,0:T(8,128)(2,1)} async-done(((bf16[128,512]{1,0:T(8,128)(2,1)}), bf16[2048,512]{1,0:T(8,128)(2,1)}) %all-gather.17.cloned.1.call-update) | async-done | bytes 2097168 | tf_op jit(solution)/shard_map/all_gather | solution.py:72
  555.1 16.1 %gather_fusion.1 = bf16[1536,2048]{1,0:T(8,128)(2,1)} fusion(bf16[1280,2048]{1,0:T(8,128)(2,1)} %bitcast.10, s32[2048]{0:T(1024)S(1)} %pad_clamp_fusion.1), kind=kCustom, calls=%fused_computation.1 | custom fusion | bytes 12589056 | tf_op jit(solution)/shard_map/gather | solution.py:107
  571.2 11.7 %reshape.194 = f32[256,6,2048]{2,1,0:T(8,128)} reshape(bf16[1536,2048]{1,0:T(8,128)(2,1)} %gather_fusion.1) | data formatting | bytes 18874368 | tf_op jit(solution)/shard_map/convert_element_type | solution.py:107
  582.9 9.4 %multiply_reduce_fusion = f32[256,2048]{1,0:T(8,128)S(1)} fusion(f32[256,6,2048]{2,1,0:T(8,128)} %reshape.194, f32[256,6]{1,0:T(8,128)S(1)} %copy.36), kind=kLoop, calls=%fused_computation.3 | loop fusion | flops 5767168 | bytes 14686208 | tf_op jit(solution)/shard_map/reduce_sum | solution.py:109
  593.7 7.3 %reduce-scatter.2.cloned.1.call-done = bf16[256,1024]{1,0:T(8,128)(2,1)} async-done(((bf16[256,2048]{1,0:T(8,128)(2,1)}), bf16[256,1024]{1,0:T(8,128)(2,1)}) %reduce-scatter.2.cloned.1.call-update) | async-done | bytes 524304 | tf_op jit(solution)/shard_map/reduce_scatter | solution.py:111
  (81 shorter events, 27.9 us)
Async XLA Ops:
  70.3 46.5 %all-to-all-start.2 = ((bf16[16,128,512]{2,1,0:T(8,128)(2,1)}), bf16[16,128,512]{2,1,0:T(8,128)(2,1)S(1)}, u32[]{:S(2)}, u32[]{:S(2)}) async-start(bf16[16,128,512]{2,1,0:T(8,128)(2,1)} %get-tuple-element.11), calls=%async_computation.2 | async-start | bytes 4194304 | tf_op jit(solution)/shard_map/all_to_all | solution.py:44
  74.3 52.5 %copy-start.10 = (s32[256,6]{0,1:T(8,128)S(1)}, s32[256,6]{0,1:T(8,128)}, u32[]{:S(2)}) copy-start(s32[256,6]{0,1:T(8,128)} %param.11) | copy-start | bytes 18436
  78.1 54.8 %copy-start.3 = (bf16[256,2048]{1,0:T(8,128)(2,1)S(1)}, bf16[256,2048]{1,0:T(8,128)(2,1)}, u32[]{:S(2)}) copy-start(bf16[256,2048]{1,0:T(8,128)(2,1)} %param.10) | copy-start | bytes 3145732
  116.8 16.4 %copy-start.1 = (bf16[16,128,512]{2,1,0:T(8,128)(2,1)}, bf16[16,128,512]{2,1,0:T(8,128)(2,1)S(1)}, u32[]{:S(2)}) copy-start(bf16[16,128,512]{2,1,0:T(8,128)(2,1)S(1)} %all-to-all-done.2) | copy-start | bytes 6291460
  116.8 52.5 %all-to-all-start.3 = ((bf16[16,128,512]{2,1,0:T(8,128)(2,1)}), bf16[16,128,512]{2,1,0:T(8,128)(2,1)}, u32[]{:S(2)}, u32[]{:S(2)}) async-start(bf16[16,128,512]{2,1,0:T(8,128)(2,1)} %convert_element_type.70), calls=%async_computation.3 | async-start | bytes 4194304 | tf_op jit(solution)/shard_map/all_to_all | solution.py:45
  126.7 58.3 %all-gather.7.cloned.1.call-start = ((), (), s32[]{:S(2)}) async-start(), calls=%async_computation.6 | async-start | bytes 6291456 | tf_op jit(solution)/shard_map/all_gather | solution.py:82
  169.3 115.4 %all-to-all-start = ((bf16[16,80,2048]{2,1,0:T(8,128)(2,1)}), bf16[16,80,2048]{2,1,0:T(8,128)(2,1)}, u32[]{:S(2)}, u32[]{:S(2)}) async-start(bf16[16,80,2048]{2,1,0:T(8,128)(2,1)} %constant_dynamic-slice_fusion), calls=%async_computation | async-start | bytes 10485760 | tf_op jit(solution)/shard_map/all_to_all | solution.py:87
  179.2 116.1 %all-gather.9.cloned.1.call-start = ((), (), s32[]{:S(2)}) async-start(), calls=%async_computation.7 | async-start | bytes 6291456 | tf_op jit(solution)/shard_map/all_gather | solution.py:83
  179.2 4.9 copy-start.8
  179.2 4.9 copy-start.9
  179.2 4.9 copy-start.12
  179.9 126.9 %all-gather.11.cloned.1.call-start = ((), (), s32[]{:S(2)}) async-start(), calls=%async_computation.8 | async-start | bytes 6291456 | tf_op jit(solution)/shard_map/all_gather | solution.py:84
  183.9 182.7 %all-gather.13.cloned.1.call-start = ((), (), s32[]{:S(2)}) async-start(), calls=%async_computation.9 | async-start | bytes 2228224 | tf_op jit(solution)/shard_map/all_gather | solution.py:70
  329.0 36.4 %copy-start.7 = (f32[128,512]{1,0:T(8,128)S(1)}, f32[128,512]{1,0:T(8,128)}, u32[]{:S(2)}) copy-start(f32[128,512]{1,0:T(8,128)} %param.19) | copy-start | bytes 786436
  329.0 37.4 %copy-start.11 = (f32[256,6]{0,1:T(8,128)S(1)}, f32[256,6]{0,1:T(8,128)}, u32[]{:S(2)}) copy-start(f32[256,6]{0,1:T(8,128)} %param.12) | copy-start | bytes 18436
  329.0 226.1 %all-to-all-start.4 = ((bf16[16,80,2048]{2,1,0:T(8,128)(2,1)}), bf16[16,80,2048]{2,1,0:T(8,128)(2,1)}, u32[]{:S(2)}, u32[]{:S(2)}) async-start(bf16[16,80,2048]{2,1,0:T(8,128)(2,1)} %bitcast.44), calls=%async_computation.4 | async-start | bytes 10485760 | tf_op jit(solution)/shard_map/all_to_all | solution.py:101
  364.8 124.4 %all-gather.15.cloned.1.call-start = ((), (), s32[]{:S(2)}) async-start(), calls=%async_computation.10 | async-start | bytes 2228224 | tf_op jit(solution)/shard_map/all_gather | solution.py:71
  365.4 186.1 %all-gather.17.cloned.1.call-start = ((), (), s32[]{:S(2)}) async-start(), calls=%async_computation.11 | async-start | bytes 2228224 | tf_op jit(solution)/shard_map/all_gather | solution.py:72
  366.1 234.9 %reduce-scatter.2.cloned.1.call-start = ((), (), s32[]{:S(2)}) async-start(), calls=%async_computation.12 | async-start | bytes 1572864 | tf_op jit(solution)/shard_map/reduce_scatter | solution.py:111
  592.3 8.7 %copy-start = (bf16[16,128,512]{2,1,0:T(8,128)(2,1)S(1)}, bf16[16,128,512]{2,1,0:T(8,128)(2,1)}, u32[]{:S(2)}) copy-start(bf16[16,128,512]{2,1,0:T(8,128)(2,1)} %all_to_all.46) | copy-start | bytes 6291460
  601.0 2.3 copy-start.2
  603.4 4.5 copy-start.4
  604.7 4.5 copy-start.5
  607.9 2.6 copy-start.6
Sparse Core Ops, SparseCore 0:
  129.1 14.9 all-gather.6
  182.1 14.8 all-gather.8
  199.2 14.8 all-gather.10
  217.2 96.2 all-gather.12
  368.6 120.5 all-gather.14
  492.4 59.0 all-gather.16
  593.8 7.1 reduce-scatter.1
where the time goes:
time: 620 us; the launch traced here: 619 us
  waiting for transfers between devices  343 us (55%)
  local copies, waits for them, and re-layouts  66.9 us (11%)
  starting transfers between devices  59.8 us (10%)
  blocking collectives  57 us (9%)
  matrix products  39 us (6%)
  other arithmetic  38.9 us (6%)
  between operations  14.5 us (2%)
    all_gather x1, waiting for transfers between devices, body(): lax.all_gather(shared_rounded[1], 'fs', axis=0, tiled=True)  120 us
    all_to_all x1, waiting for transfers between devices, body(): lax.all_to_all(own_share, 'fs', split_axis=0, concat_axis=0, tiled=True)  99.7 us
    all_gather x1, waiting for transfers between devices, body(): lax.all_gather(shared_rounded[2], 'fs', axis=0, tiled=True)  62.3 us
    all_to_all x1, blocking collectives, body(): lax.all_to_all(rounded[0], 'fs', split_axis=0, concat_axis=1, tiled=True)  57 us
    all_to_all x1, waiting for transfers between devices, body(): lax.all_to_all(rounded[1], 'fs', split_axis=0, concat_axis=1, tiled=True)  38.7 us
    all_to_all x1, starting transfers between devices, body(): lax.all_to_all(results, 'fs', split_axis=0, concat_axis=0, tiled=True)  35.7 us
    gather x1, local copies, waits for them, and re-layouts, body(): taken = back[local].astype(jnp.float32).reshape(tok_rows, picks, width)  16.1 us
    all_to_all x1, waiting for transfers between devices, body(): lax.all_to_all(rounded[2], 'fs', split_axis=0, concat_axis=1, tiled=True)  12.7 us
  transfers between devices with their start and end apart: 11, of which 6 were waited for; matrix products, arithmetic and copies ran while one was open for 14% of the time, Pallas kernels for 0%

commit v1 on v0

--- a/solution.py
+++ b/solution.py
@@ -4,6 +4,19 @@
 from jax.sharding import PartitionSpec as P
 
 EPSILON = 1e-06
+
+
+def collect(x, axis, dim):
+    ways = lax.axis_size(axis)
+    up = [(d, (d + 1) % ways) for d in range(ways)]
+    down = [(d, (d - 1) % ways) for d in range(ways)]
+    earlier, later = ([x], [x])
+    for _ in range(ways // 2):
+        earlier.append(lax.ppermute(earlier[-1], axis, up))
+    for _ in range((ways - 1) // 2):
+        later.append(lax.ppermute(later[-1], axis, down))
+    line = jnp.concatenate([*earlier[::-1], *later[1:]], axis=dim)
+    return jnp.roll(line, (lax.axis_index(axis) - ways // 2) * x.shape[dim], axis=dim)
 
 
 def normalize(tokens):
@@ -68,7 +81,7 @@
     )
     common_gate, common_up, common_down = (
         lax.all_gather(shared_rounded[0], "fs", axis=0, tiled=True),
-        lax.all_gather(shared_rounded[1], "fs", axis=0, tiled=True),
+        collect(shared_rounded[1], "fs", 0),
         lax.all_gather(shared_rounded[2], "fs", axis=0, tiled=True),
     )
     shared_gate_act = jnp.dot(normed, common_gate, preferred_element_type=jnp.float32)

time: 620 us -> 644 us (1.039)
  starting transfers between devices: 59.8 us -> 95.5 us
  waiting for transfers between devices: 343 us -> 329 us
    ppermute x0 -> x15, waiting for transfers between devices: none -> 127 us  [the longest x8 112 us: collect(): earlier.append(lax.ppermute(earlier[-1], axis, up))]
    all_gather x1 -> x0, waiting for transfers between devices: 120 us -> none  [body(): lax.all_gather(shared_rounded[1], 'fs', axis=0, tiled=True)]
    ppermute x0 -> x15, starting transfers between devices: none -> 47.2 us  [the longest x7 42.7 us: collect(): later.append(lax.ppermute(later[-1], axis, down))]
    all_to_all x1, waiting for transfers between devices: 99.7 us -> 80 us  [body(): lax.all_to_all(own_share, 'fs', split_axis=0, concat_axis=0, tiled=True)]
    all_gather x1, waiting for transfers between devices: 62.3 us -> 50.5 us  [body(): lax.all_gather(shared_rounded[2], 'fs', axis=0, tiled=True)]
    all_gather x1, waiting for transfers between devices: 0.02 us -> 11.6 us  [body(): lax.all_gather(gate_rows, 'tp', axis=1, tiled=True)]
    all_to_all x1, starting transfers between devices: 35.7 us -> 24.3 us  [body(): lax.all_to_all(results, 'fs', split_axis=0, concat_axis=0, tiled=True)]
  transfers between devices with their start and end apart: 11 -> 25, of which waited for: 6 -> 17; matrix products, arithmetic and copies ran while one was open for 14% -> 11% of each run, Pallas kernels for 0% -> 0%
where the time goes in v1:
time: 644 us; the launch traced here: 643 us
  waiting for transfers between devices  329 us (51%)
  starting transfers between devices  95.5 us (15%)
  local copies, waits for them, and re-layouts  67.7 us (11%)
  blocking collectives  57 us (9%)
  other arithmetic  38.9 us (6%)
  matrix products  38.9 us (6%)
  between operations  15.9 us (2%)
    ppermute x8, waiting for transfers between devices, collect(): earlier.append(lax.ppermute(earlier[-1], axis, up))  112 us
    all_to_all x1, waiting for transfers between devices, body(): lax.all_to_all(own_share, 'fs', split_axis=0, concat_axis=0, tiled=True)  80 us
    all_to_all x1, blocking collectives, body(): lax.all_to_all(rounded[0], 'fs', split_axis=0, concat_axis=1, tiled=True)  57 us
    all_gather x1, waiting for transfers between devices, body(): lax.all_gather(shared_rounded[2], 'fs', axis=0, tiled=True)  50.5 us
    ppermute x7, starting transfers between devices, collect(): later.append(lax.ppermute(later[-1], axis, down))  42.7 us
    all_to_all x1, waiting for transfers between devices, body(): lax.all_to_all(rounded[1], 'fs', split_axis=0, concat_axis=1, tiled=True)  38.7 us
    all_to_all x1, starting transfers between devices, body(): lax.all_to_all(results, 'fs', split_axis=0, concat_axis=0, tiled=True)  24.3 us
    gather x1, local copies, waits for them, and re-layouts, body(): taken = back[local].astype(jnp.float32).reshape(tok_rows, picks, width)  16.1 us
  transfers between devices with their start and end apart: 25, of which 17 were waited for; matrix products, arithmetic and copies ran while one was open for 11% of the time, Pallas kernels for 0%

profile of v1, /device:TPU:0, one launch (start us, length us, event | category | flops | bytes accessed | tf_op | source)
XLA Modules:
  0.0 642.5 jit_solution(8065882567579183464)
XLA Ops:
  8.0 6.1 multiply_convert_fusion.1
  14.1 57.0 %all_to_all.46 = bf16[16,128,512]{2,1,0:T(8,128)(2,1)} all-to-all(bf16[16,128,512]{2,1,0:T(8,128)(2,1)S(1)} %get-tuple-element.12), channel_id=1, replica_groups=mesh['fs'=16,'tp'=2] {'fs'}, dimensions={0} | all-to-all | bytes 4194304 | tf_op jit(solution)/shard_map/all_to_all | solution.py:56
  78.9 38.7 %all-to-all-done.2 = bf16[16,128,512]{2,1,0:T(8,128)(2,1)S(1)} async-done(((bf16[16,128,512]{2,1,0:T(8,128)(2,1)}), bf16[16,128,512]{2,1,0:T(8,128)(2,1)S(1)}, u32[]{:S(2)}, u32[]{:S(2)}) %all-to-all-start.2) | async-done | bytes 2097184 | tf_op jit(solution)/shard_map/all_to_all | solution.py:57
  117.7 9.9 %all-to-all-start.3 = ((bf16[16,128,512]{2,1,0:T(8,128)(2,1)}), bf16[16,128,512]{2,1,0:T(8,128)(2,1)}, u32[]{:S(2)}, u32[]{:S(2)}) async-start(bf16[16,128,512]{2,1,0:T(8,128)(2,1)} %convert_element_type.70), calls=%async_computation.3 | async-start | bytes 4194304 | tf_op jit(solution)/shard_map/all_to_all | solution.py:58
  135.3 6.2 scatter_custom_fusion
  141.5 10.9 %gather_fusion = bf16[2560,2048]{1,0:T(8,128)(2,1)} fusion(bf16[257,2048]{1,0:T(8,128)(2,1)S(1)} %concatenate.9, s32[3072]{0:T(1024)S(1)} %pad_clamp_fusion), kind=kCustom, calls=%fused_computation | custom fusion | bytes 20981760 | tf_op jit(solution)/shard_map/gather | solution.py:76
  158.1 12.1 %all-to-all-done.3 = bf16[16,128,512]{2,1,0:T(8,128)(2,1)} async-done(((bf16[16,128,512]{2,1,0:T(8,128)(2,1)}), bf16[16,128,512]{2,1,0:T(8,128)(2,1)}, u32[]{:S(2)}, u32[]{:S(2)}) %all-to-all-start.3) | async-done | bytes 2097184 | tf_op jit(solution)/shard_map/all_to_all | solution.py:58
  170.2 9.8 %all-to-all-start = ((bf16[16,80,2048]{2,1,0:T(8,128)(2,1)}), bf16[16,80,2048]{2,1,0:T(8,128)(2,1)}, u32[]{:S(2)}, u32[]{:S(2)}) async-start(bf16[16,80,2048]{2,1,0:T(8,128)(2,1)} %constant_dynamic-slice_fusion.1), calls=%async_computation | async-start | bytes 10485760 | tf_op jit(solution)/shard_map/all_to_all | solution.py:100
  185.7 11.6 %all-gather.6.cloned.1.call-done = bf16[2048,1024]{1,0:T(8,128)(2,1)} async-done(((bf16[2048,512]{1,0:T(8,128)(2,1)}), bf16[2048,1024]{1,0:T(8,128)(2,1)}) %all-gather.6.cloned.1.call-update) | async-done | bytes 4194320 | tf_op jit(solution)/shard_map/all_gather | solution.py:95
  197.3 80.0 %all-to-all-done = bf16[16,80,2048]{2,1,0:T(8,128)(2,1)} async-done(((bf16[16,80,2048]{2,1,0:T(8,128)(2,1)}), bf16[16,80,2048]{2,1,0:T(8,128)(2,1)}, u32[]{:S(2)}, u32[]{:S(2)}) %all-to-all-start) | async-done | bytes 5242912 | tf_op jit(solution)/shard_map/all_to_all | solution.py:100
  277.3 10.6 %fusion.27 = f32[1280,1024]{0,1:T(8,128)} fusion(bf16[1280,2048]{1,0:T(8,128)(2,1)} %bitcast.2, bf16[2048,1024]{1,0:T(8,128)(2,1)} %all-gather.6.cloned.1.call-done), kind=kOutput, calls=%fused_computation.101 | convolution fusion | flops 5368709120 | bytes 14680064 | tf_op jit(solution)/shard_map/dot_general | solution.py:102
  287.9 10.4 %multiply_convert_fusion = bf16[1280,1024]{0,1:T(8,128)(2,1)S(1)} fusion(f32[1280,1024]{0,1:T(8,128)} %fusion.27, bf16[1280,2048]{1,0:T(8,128)(2,1)} %bitcast.2, bf16[2048,1024]{1,0:T(8,128)(2,1)} %all-gather.8.cloned.1.call-done), kind=kOutput, calls=%fused_computation.6 | convolution fusion | flops 5376573440 | bytes 17301504 | tf_op jit(solution)/shard_map/dot_general | solution.py:103
  298.4 10.6 %fusion = bf16[1280,2,2048]{2,0,1:T(8,128)(2,1)} fusion(bf16[1280,2,512]{0,2,1:T(8,128)(2,1)S(1)} %bitcast.52, bf16[2048,2,512]{0,2,1:T(8,128)(2,1)} %bitcast.51), kind=kOutput, calls=%fused_computation.5 | convolution fusion | flops 5373952000 | bytes 17301504 | tf_op jit(solution)/shard_map/rbf,dbf->rbd/dot_general | solution.py:105
  309.0 11.2 %reduce_sum.46 = bf16[1280,2048]{1,0:T(8,128)(2,1)} reduce(bf16[1280,2,2048]{2,0,1:T(8,128)(2,1)} %fusion, bf16[]{:T(256)} %constant.86.clone.1), dimensions={1}, to_apply=%region_5.6 | reduce | flops 2621440 | bytes 15728642 | tf_op jit(solution)/shard_map/reduce_sum | solution.py:112
  320.2 24.3 %all-to-all-start.4 = ((bf16[16,80,2048]{2,1,0:T(8,128)(2,1)}), bf16[16,80,2048]{2,1,0:T(8,128)(2,1)}, u32[]{:S(2)}, u32[]{:S(2)}) async-start(bf16[16,80,2048]{2,1,0:T(8,128)(2,1)} %bitcast.44), calls=%async_computation.4 | async-start | bytes 10485760 | tf_op jit(solution)/shard_map/all_to_all | solution.py:114
  347.3 99.3 %collective-permute-done = bf16[128,512]{1,0:T(8,128)(2,1)S(1)} collective-permute-done((bf16[128,512]{1,0:T(8,128)(2,1)S(1)}, bf16[128,512]{1,0:T(8,128)(2,1)S(1)}, u32[]{:S(2)}, u32[]{:S(2)}) %collective-permute-start) | collective-permute-done | bytes 131104 | tf_op jit(solution)/shard_map/ppermute | solution.py:15
  460.6 8.7 %collective-permute-start.9 = (bf16[128,512]{1,0:T(8,128)(2,1)S(1)}, bf16[128,512]{1,0:T(8,128)(2,1)S(1)}, u32[]{:S(2)}, u32[]{:S(2)}) collective-permute-start(bf16[128,512]{1,0:T(8,128)(2,1)S(1)} %collective-permute-done.8), channel_id=1, source_target_pairs={{0,30},{2,0},{4,2},{6,4},{8,6},{10,8},{12,10},{14,12},{16,14},{18,... | collective-permute-start | bytes 393224 | tf_op jit(solution)/shard_map/ppermute | solution.py:17
  469.3 6.1 collective-permute-done.9
  495.2 6.1 collective-permute-start.12
  525.4 50.5 %all-gather.14.cloned.1.call-done = bf16[2048,512]{1,0:T(8,128)(2,1)} async-done(((bf16[128,512]{1,0:T(8,128)(2,1)}), bf16[2048,512]{1,0:T(8,128)(2,1)}) %all-gather.14.cloned.1.call-update) | async-done | bytes 2097168 | tf_op jit(solution)/shard_map/all_gather | solution.py:85
  580.0 16.1 %gather_fusion.1 = bf16[1536,2048]{1,0:T(8,128)(2,1)} fusion(bf16[1280,2048]{1,0:T(8,128)(2,1)} %bitcast.10, s32[2048]{0:T(1024)S(1)} %pad_clamp_fusion.1), kind=kCustom, calls=%fused_computation.1 | custom fusion | bytes 12589056 | tf_op jit(solution)/shard_map/gather | solution.py:120
  596.1 11.7 %reshape.194 = f32[256,6,2048]{2,1,0:T(8,128)} reshape(bf16[1536,2048]{1,0:T(8,128)(2,1)} %gather_fusion.1) | data formatting | bytes 18874368 | tf_op jit(solution)/shard_map/convert_element_type | solution.py:120
  607.8 9.5 %multiply_reduce_fusion = f32[256,2048]{1,0:T(8,128)S(1)} fusion(f32[256,6,2048]{2,1,0:T(8,128)} %reshape.194, f32[256,6]{1,0:T(8,128)S(1)} %copy.36), kind=kLoop, calls=%fused_computation.3 | loop fusion | flops 5767168 | bytes 14686208 | tf_op jit(solution)/shard_map/reduce_sum | solution.py:122
  618.6 7.3 %reduce-scatter.2.cloned.1.call-done = bf16[256,1024]{1,0:T(8,128)(2,1)} async-done(((bf16[256,2048]{1,0:T(8,128)(2,1)}), bf16[256,1024]{1,0:T(8,128)(2,1)}) %reduce-scatter.2.cloned.1.call-update) | async-done | bytes 524304 | tf_op jit(solution)/shard_map/reduce_scatter | solution.py:124
  (146 shorter events, 101.9 us)
Async XLA Ops:
  71.2 46.5 %all-to-all-start.2 = ((bf16[16,128,512]{2,1,0:T(8,128)(2,1)}), bf16[16,128,512]{2,1,0:T(8,128)(2,1)S(1)}, u32[]{:S(2)}, u32[]{:S(2)}) async-start(bf16[16,128,512]{2,1,0:T(8,128)(2,1)} %get-tuple-element.11), calls=%async_computation.2 | async-start | bytes 4194304 | tf_op jit(solution)/shard_map/all_to_all | solution.py:57
  117.7 52.5 %all-to-all-start.3 = ((bf16[16,128,512]{2,1,0:T(8,128)(2,1)}), bf16[16,128,512]{2,1,0:T(8,128)(2,1)}, u32[]{:S(2)}, u32[]{:S(2)}) async-start(bf16[16,128,512]{2,1,0:T(8,128)(2,1)} %convert_element_type.70), calls=%async_computation.3 | async-start | bytes 4194304 | tf_op jit(solution)/shard_map/all_to_all | solution.py:58
  170.2 107.1 %all-to-all-start = ((bf16[16,80,2048]{2,1,0:T(8,128)(2,1)}), bf16[16,80,2048]{2,1,0:T(8,128)(2,1)}, u32[]{:S(2)}, u32[]{:S(2)}) async-start(bf16[16,80,2048]{2,1,0:T(8,128)(2,1)} %constant_dynamic-slice_fusion.1), calls=%async_computation | async-start | bytes 10485760 | tf_op jit(solution)/shard_map/all_to_all | solution.py:100
  180.0 17.3 %all-gather.6.cloned.1.call-start = ((), (), s32[]{:S(2)}) async-start(), calls=%async_computation.6 | async-start | bytes 6291456 | tf_op jit(solution)/shard_map/all_gather | solution.py:95
  180.7 107.1 %all-gather.8.cloned.1.call-start = ((), (), s32[]{:S(2)}) async-start(), calls=%async_computation.7 | async-start | bytes 6291456 | tf_op jit(solution)/shard_map/all_gather | solution.py:96
  181.5 116.9 %all-gather.10.cloned.1.call-start = ((), (), s32[]{:S(2)}) async-start(), calls=%async_computation.8 | async-start | bytes 6291456 | tf_op jit(solution)/shard_map/all_gather | solution.py:97
  320.2 259.7 %all-to-all-start.4 = ((bf16[16,80,2048]{2,1,0:T(8,128)(2,1)}), bf16[16,80,2048]{2,1,0:T(8,128)(2,1)}, u32[]{:S(2)}, u32[]{:S(2)}) async-start(bf16[16,80,2048]{2,1,0:T(8,128)(2,1)} %bitcast.44), calls=%async_computation.4 | async-start | bytes 10485760 | tf_op jit(solution)/shard_map/all_to_all | solution.py:114
  344.5 177.0 %all-gather.12.cloned.1.call-start = ((), (), s32[]{:S(2)}) async-start(), calls=%async_computation.9 | async-start | bytes 2228224 | tf_op jit(solution)/shard_map/all_gather | solution.py:83
  345.4 230.5 %all-gather.14.cloned.1.call-start = ((), (), s32[]{:S(2)}) async-start(), calls=%async_computation.10 | async-start | bytes 2228224 | tf_op jit(solution)/shard_map/all_gather | solution.py:85
  345.4 101.2 %collective-permute-start = (bf16[128,512]{1,0:T(8,128)(2,1)S(1)}, bf16[128,512]{1,0:T(8,128)(2,1)S(1)}, u32[]{:S(2)}, u32[]{:S(2)}) collective-permute-start(bf16[128,512]{1,0:T(8,128)(2,1)S(1)} %get-tuple-element.10), channel_id=1, source_target_pairs={{0,2},{2,4},{4,6},{6,8},{8,10},{10,12},{12,14},{14,16},{16,18},{18... | collective-permute-start | bytes 393224 | tf_op jit(solution)/shard_map/ppermute | solution.py:15
  446.6 11.5 %collective-permute-start.1 = (bf16[128,512]{1,0:T(8,128)(2,1)S(1)}, bf16[128,512]{1,0:T(8,128)(2,1)S(1)}, u32[]{:S(2)}, u32[]{:S(2)}) collective-permute-start(bf16[128,512]{1,0:T(8,128)(2,1)S(1)} %collective-permute-done), channel_id=1, source_target_pairs={{0,2},{2,4},{4,6},{6,8},{8,10},{10,12},{12,14},{14,16},{16,18},{18... | collective-permute-start | bytes 393224 | tf_op jit(solution)/shard_map/ppermute | solution.py:15
  446.6 14.0 %collective-permute-start.8 = (bf16[128,512]{1,0:T(8,128)(2,1)S(1)}, bf16[128,512]{1,0:T(8,128)(2,1)S(1)}, u32[]{:S(2)}, u32[]{:S(2)}) collective-permute-start(bf16[128,512]{1,0:T(8,128)(2,1)S(1)} %get-tuple-element.10), channel_id=1, source_target_pairs={{0,30},{2,0},{4,2},{6,4},{8,6},{10,8},{12,10},{14,12},{16,14},{18,... | collective-permute-start | bytes 393224 | tf_op jit(solution)/shard_map/ppermute | solution.py:17
  458.1 11.1 %collective-permute-start.2 = (bf16[128,512]{1,0:T(8,128)(2,1)S(1)}, bf16[128,512]{1,0:T(8,128)(2,1)S(1)}, u32[]{:S(2)}, u32[]{:S(2)}) collective-permute-start(bf16[128,512]{1,0:T(8,128)(2,1)S(1)} %collective-permute-done.1), channel_id=1, source_target_pairs={{0,2},{2,4},{4,6},{6,8},{8,10},{10,12},{12,14},{14,16},{16,18},{18... | collective-permute-start | bytes 393224 | tf_op jit(solution)/shard_map/ppermute | solution.py:15
  460.6 14.8 %collective-permute-start.9 = (bf16[128,512]{1,0:T(8,128)(2,1)S(1)}, bf16[128,512]{1,0:T(8,128)(2,1)S(1)}, u32[]{:S(2)}, u32[]{:S(2)}) collective-permute-start(bf16[128,512]{1,0:T(8,128)(2,1)S(1)} %collective-permute-done.8), channel_id=1, source_target_pairs={{0,30},{2,0},{4,2},{6,4},{8,6},{10,8},{12,10},{14,12},{16,14},{18,... | collective-permute-start | bytes 393224 | tf_op jit(solution)/shard_map/ppermute | solution.py:17
  469.3 12.2 %collective-permute-start.3 = (bf16[128,512]{1,0:T(8,128)(2,1)S(1)}, bf16[128,512]{1,0:T(8,128)(2,1)S(1)}, u32[]{:S(2)}, u32[]{:S(2)}) collective-permute-start(bf16[128,512]{1,0:T(8,128)(2,1)S(1)} %collective-permute-done.2), channel_id=1, source_target_pairs={{0,2},{2,4},{4,6},{6,8},{8,10},{10,12},{12,14},{14,16},{16,18},{18... | collective-permute-start | bytes 393224 | tf_op jit(solution)/shard_map/ppermute | solution.py:15
  475.4 11.2 %collective-permute-start.10 = (bf16[128,512]{1,0:T(8,128)(2,1)S(1)}, bf16[128,512]{1,0:T(8,128)(2,1)S(1)}, u32[]{:S(2)}, u32[]{:S(2)}) collective-permute-start(bf16[128,512]{1,0:T(8,128)(2,1)S(1)} %collective-permute-done.9), channel_id=1, source_target_pairs={{0,30},{2,0},{4,2},{6,4},{8,6},{10,8},{12,10},{14,12},{16,14},{18,... | collective-permute-start | bytes 393224 | tf_op jit(solution)/shard_map/ppermute | solution.py:17
  481.5 12.4 %collective-permute-start.4 = (bf16[128,512]{1,0:T(8,128)(2,1)S(1)}, bf16[128,512]{1,0:T(8,128)(2,1)S(1)}, u32[]{:S(2)}, u32[]{:S(2)}) collective-permute-start(bf16[128,512]{1,0:T(8,128)(2,1)S(1)} %collective-permute-done.3), channel_id=1, source_target_pairs={{0,2},{2,4},{4,6},{6,8},{8,10},{10,12},{12,14},{14,16},{16,18},{18... | collective-permute-start | bytes 393224 | tf_op jit(solution)/shard_map/ppermute | solution.py:15
  486.6 8.6 %collective-permute-start.11 = (bf16[128,512]{1,0:T(8,128)(2,1)S(1)}, bf16[128,512]{1,0:T(8,128)(2,1)S(1)}, u32[]{:S(2)}, u32[]{:S(2)}) collective-permute-start(bf16[128,512]{1,0:T(8,128)(2,1)S(1)} %collective-permute-done.10), channel_id=1, source_target_pairs={{0,30},{2,0},{4,2},{6,4},{8,6},{10,8},{12,10},{14,12},{16,14},{18,... | collective-permute-start | bytes 393224 | tf_op jit(solution)/shard_map/ppermute | solution.py:17
  493.9 9.2 %collective-permute-start.5 = (bf16[128,512]{1,0:T(8,128)(2,1)S(1)}, bf16[128,512]{1,0:T(8,128)(2,1)S(1)}, u32[]{:S(2)}, u32[]{:S(2)}) collective-permute-start(bf16[128,512]{1,0:T(8,128)(2,1)S(1)} %collective-permute-done.4), channel_id=1, source_target_pairs={{0,2},{2,4},{4,6},{6,8},{8,10},{10,12},{12,14},{14,16},{16,18},{18... | collective-permute-start | bytes 393224 | tf_op jit(solution)/shard_map/ppermute | solution.py:15
  495.2 8.9 %collective-permute-start.12 = (bf16[128,512]{1,0:T(8,128)(2,1)S(1)}, bf16[128,512]{1,0:T(8,128)(2,1)S(1)}, u32[]{:S(2)}, u32[]{:S(2)}) collective-permute-start(bf16[128,512]{1,0:T(8,128)(2,1)S(1)} %collective-permute-done.11), channel_id=1, source_target_pairs={{0,30},{2,0},{4,2},{6,4},{8,6},{10,8},{12,10},{14,12},{16,14},{18,... | collective-permute-start | bytes 393224 | tf_op jit(solution)/shard_map/ppermute | solution.py:17
  503.1 8.6 %collective-permute-start.6 = (bf16[128,512]{1,0:T(8,128)(2,1)S(1)}, bf16[128,512]{1,0:T(8,128)(2,1)S(1)}, u32[]{:S(2)}, u32[]{:S(2)}) collective-permute-start(bf16[128,512]{1,0:T(8,128)(2,1)S(1)} %collective-permute-done.5), channel_id=1, source_target_pairs={{0,2},{2,4},{4,6},{6,8},{8,10},{10,12},{12,14},{14,16},{16,18},{18... | collective-permute-start | bytes 393224 | tf_op jit(solution)/shard_map/ppermute | solution.py:15
  503.8 122.1 %reduce-scatter.2.cloned.1.call-start = ((), (), s32[]{:S(2)}) async-start(), calls=%async_computation.11 | async-start | bytes 1572864 | tf_op jit(solution)/shard_map/reduce_scatter | solution.py:124
  504.1 10.1 %collective-permute-start.13 = (bf16[128,512]{1,0:T(8,128)(2,1)S(1)}, bf16[128,512]{1,0:T(8,128)(2,1)S(1)}, u32[]{:S(2)}, u32[]{:S(2)}) collective-permute-start(bf16[128,512]{1,0:T(8,128)(2,1)S(1)} %collective-permute-done.12), channel_id=1, source_target_pairs={{0,30},{2,0},{4,2},{6,4},{8,6},{10,8},{12,10},{14,12},{16,14},{18,... | collective-permute-start | bytes 393224 | tf_op jit(solution)/shard_map/ppermute | solution.py:17
  511.7 8.7 %collective-permute-start.7 = (bf16[128,512]{1,0:T(8,128)(2,1)S(1)}, bf16[128,512]{1,0:T(8,128)(2,1)S(1)}, u32[]{:S(2)}, u32[]{:S(2)}) collective-permute-start(bf16[128,512]{1,0:T(8,128)(2,1)S(1)} %collective-permute-done.6), channel_id=1, source_target_pairs={{0,2},{2,4},{4,6},{6,8},{8,10},{10,12},{12,14},{14,16},{16,18},{18... | collective-permute-start | bytes 393224 | tf_op jit(solution)/shard_map/ppermute | solution.py:15
  (17 other events, 667.7 us)
Sparse Core Ops, SparseCore 0:
  182.3 14.8 all-gather.5
  199.4 14.8 all-gather.7
  216.4 14.8 all-gather.9
  618.7 7.1 reduce-scatter.1
Sparse Core Ops, SparseCore 1:
  348.3 142.1 all-gather.11
  503.9 71.9 all-gather.13
